TPU v7x, 32 devices: a whole 2x2x4 slice. The times are simulated.
32 devices in a mesh: dp: 4 (over y, x), kv: 4 (over z), tp: 2 (over core).
Axes of the slice: x: 2, y: 2, z: 4, core: 2. Of those that a mesh axis runs over, the one named last changes fastest.
Arguments:
- tokens: bfloat16 [4096, 4096], P(('dp', 'kv')), parts along dimension 0, may hold values from -16 to 16
- query_weight: bfloat16 [4096, 1024], P('kv', 'tp'), may hold values from -0.09375 to 0.09375
- key_weight: bfloat16 [4096, 256], P('kv', 'tp'), may hold values from -0.09375 to 0.09375
- value_weight: bfloat16 [4096, 256], P('kv', 'tp'), may hold values from -0.09375 to 0.09375
- out_weight: bfloat16 [1024, 4096], P('kv', 'tp'), may hold values from -1.5 to 1.5
- chosen: int32 [128, 16], P(('dp', 'kv')), parts along dimension 0, may hold values from -1 to 31, as said below
- live_length: int32 [4], P('dp'), parts along dimension 0, may hold values from 128 to 1024
Outputs:
- mixed: bfloat16 [4096, 4096], P(('dp', 'kv'), 'tp'), parts along dimension 0
There are 4 independent parts, one for each index of `dp`. A program takes and returns all parts, laid end to end along the dimension named above; an argument that names none is the same for every part. Nothing has to cross between parts.
Inputs may be any that keep to these rules, and one draw needn't show every extreme that they name: `chosen`: row j lists 16 entries: entry 0 is j itself, the others are distinct blocks before j, or -1 for unused entries. The query blocks of one device together read at most 2 distinct blocks held by any one other device, and some device reads 2 of another's in every draw.
All inputs are finite; a program needn't handle non-finite values.
Results may differ from a plain program's by a relative error of at most 0.0085.
Values may be sent and summed in bfloat16 or wider, within the bound.
A program may use at most 64 MiB of HBM per device.

v0:
```python
import jax
import jax.numpy as jnp
from jax import lax
from jax.sharding import PartitionSpec as P

HD = 128
BLOCK = 32
CAP = 2


def body(tokens, query_weight, key_weight, value_weight, out_weight, chosen, live_length):
    rows = tokens.shape[0]
    per_dev = rows // BLOCK
    owners = lax.axis_size("kv")
    me = lax.axis_index("kv")

    def add_rows(piece):
        return jnp.dot(tokens, piece, preferred_element_type=jnp.float32)

    queries = add_rows(lax.all_gather(query_weight, "kv", axis=0, tiled=True))
    keys = add_rows(lax.all_gather(key_weight, "kv", axis=0, tiled=True))
    values = add_rows(lax.all_gather(value_weight, "kv", axis=0, tiled=True))
    queries = queries.astype(jnp.bfloat16)
    paired = jnp.concatenate([keys.astype(jnp.bfloat16), values.astype(jnp.bfloat16)], axis=1)
    width = paired.shape[1]
    local_blocks = paired.reshape(per_dev, BLOCK, width)
    valid = chosen >= 0
    safe = jnp.maximum(chosen, 0)
    blocks_all = owners * per_dev
    hits = (safe[:, :, None] == jnp.arange(blocks_all, dtype=jnp.int32)[None, None, :]) & valid[
        :, :, None
    ]
    needed = jnp.any(hits, axis=(0, 1)).reshape(owners, per_dev)
    needed = needed & (jnp.arange(owners, dtype=jnp.int32) != me)[:, None]
    ranks = jnp.cumsum(needed.astype(jnp.int32), axis=1)
    local_ids = jnp.arange(per_dev, dtype=jnp.int32)
    slot_lists = []
    for slot in range(CAP):
        marked = needed & (ranks == slot + 1)
        found = jnp.any(marked, axis=1)
        where_at = jnp.sum(jnp.where(marked, local_ids[None, :], 0), axis=1)
        slot_lists.append(jnp.where(found, where_at, -1))
    wanted = jnp.stack(slot_lists, axis=1)
    requested = lax.all_to_all(wanted, "kv", split_axis=0, concat_axis=0, tiled=True)
    outgoing = local_blocks[jnp.maximum(requested, 0)]
    outgoing = jnp.where((requested >= 0)[:, :, None, None], outgoing, jnp.zeros((), jnp.bfloat16))
    incoming = lax.all_to_all(outgoing, "kv", split_axis=0, concat_axis=0, tiled=True)
    table = jnp.concatenate([incoming.reshape(owners * CAP, BLOCK, width), local_blocks], axis=0)
    segment_retainer = safe // per_dev
    local_of = safe % per_dev
    match = (wanted[None, None, :, :] == local_of[:, :, None, None]) & (
        jnp.arange(owners, dtype=jnp.int32)[None, None, :, None]
        == segment_retainer[:, :, None, None]
    )
    slot_index = jnp.arange(owners * CAP, dtype=jnp.int32).reshape(owners, CAP)
    remote_at = jnp.sum(jnp.where(match, slot_index[None, None], 0), axis=(2, 3))
    position = jnp.where(segment_retainer == me, owners * CAP + local_of, remote_at)
    picked = table[position]
    near_keys = picked[..., :HD]
    near_values = picked[..., HD:]
    grouped = queries.reshape(per_dev, BLOCK, -1, HD)
    scores = jnp.einsum(
        "jqhd,jnbd->jhqnb", grouped, near_keys, preferred_element_type=jnp.float32
    ) * HD ** (-0.5)
    query_pos = (me * per_dev + jnp.arange(per_dev, dtype=jnp.int32))[:, None] * BLOCK + jnp.arange(
        BLOCK, dtype=jnp.int32
    )[None, :]
    key_pos = safe[:, :, None] * BLOCK + jnp.arange(BLOCK, dtype=jnp.int32)[None, None, :]
    allowed = valid[:, None, :, None] & (key_pos[:, None, :, :] <= query_pos[:, :, None, None])
    masked = jnp.where(allowed[:, None], scores, -jnp.inf)
    top = jnp.max(masked, axis=(3, 4), keepdims=True)
    weights = jnp.exp(masked - top)
    total = jnp.sum(weights, axis=(3, 4))
    summed = jnp.einsum(
        "jhqnb,jnbd->jqhd",
        weights.astype(jnp.bfloat16),
        near_values,
        preferred_element_type=jnp.float32,
    )
    result = summed / jnp.transpose(total, (0, 2, 1))[..., None]
    live = query_pos < live_length[0]
    result = jnp.where(live[:, :, None, None], result, 0.0)
    attended = result.astype(jnp.bfloat16).reshape(rows, -1)
    every_head = lax.all_gather(attended, "tp", axis=1, tiled=True)
    mixed = jnp.dot(
        every_head,
        lax.all_gather(out_weight, "kv", axis=0, tiled=True),
        preferred_element_type=jnp.float32,
    )
    return mixed.astype(jnp.bfloat16)


def solution(mesh):
    in_specs = (
        P(("dp", "kv"), None),
        P("kv", "tp"),
        P("kv", "tp"),
        P("kv", "tp"),
        P("kv", "tp"),
        P(("dp", "kv"), None),
        P("dp"),
    )
    out_specs = P(("dp", "kv"), "tp")
    return jax.shard_map(body, mesh=mesh, in_specs=in_specs, out_specs=out_specs, check_vma=False)
```

profile of v0, /device:TPU:0, one launch (start us, length us, event | category | flops | bytes accessed | tf_op | source)
XLA Modules:
  0.0 241.9 jit_solution(13288918027579121998)
XLA Ops:
  6.5 0.0 copy-start
  6.5 0.0 all-gather.7.cloned.1.call-start
  6.5 0.7 all-gather.7.cloned.1.call-update
  7.3 0.0 all-gather.5.cloned.1.call-start
  7.3 0.7 all-gather.5.cloned.1.call-update
  8.0 0.0 all-gather.9.cloned.1.call-start
  8.1 0.7 all-gather.9.cloned.1.call-update
  8.7 0.0 all-gather.11.cloned.1.call-start
  8.8 0.5 all-gather.11.cloned.1.call-update
  9.3 0.7 add_select_fusion.1
  10.0 0.7 broadcast_compare_fusion
  10.7 0.1 fusion.21
  10.8 0.1 reshape.143
  10.9 0.1 fusion.26
  11.0 0.2 reduce_window_sum.11
  11.2 0.2 select_reduce_fusion.2
  11.4 0.1 reduce_or.28
  11.5 0.1 reduce_or.29
  11.6 0.7 copy.33
  12.3 6.3 %all-to-all-start = ((s32[4,1,2]{2,1,0:T(1,128)}), s32[4,1,2]{2,1,0:T(1,128)S(1)}, u32[]{:S(2)}, u32[]{:S(2)}) async-start(s32[4,1,2]{2,1,0:T(1,128)} %copy.33), calls=%async_computation | async-start | bytes 4096 | tf_op jit(solution)/shard_map/all_to_all | solution.py:44
  18.7 0.1 copy.35
  18.8 0.1 select_reduce_fusion
  18.8 0.7 broadcast_multiply_fusion
  19.5 0.1 reshape.158
  20.3 0.1 iota_add_fusion.1
  20.4 0.1 iota_add_fusion
  20.5 1.0 compare_and_fusion
  21.5 2.7 %all-to-all-done = s32[4,1,2]{2,1,0:T(1,128)S(1)} async-done(((s32[4,1,2]{2,1,0:T(1,128)}), s32[4,1,2]{2,1,0:T(1,128)S(1)}, u32[]{:S(2)}, u32[]{:S(2)}) %all-to-all-start) | async-done | bytes 64 | tf_op jit(solution)/shard_map/all_to_all | solution.py:44
  24.2 0.1 reshape.150
  24.3 15.4 %all-gather.7.cloned.1.call-done = bf16[4096,128]{1,0:T(8,128)(2,1)} async-done(((bf16[1024,128]{1,0:T(8,128)(2,1)}), bf16[4096,128]{1,0:T(8,128)(2,1)}) %all-gather.7.cloned.1.call-update) | async-done | bytes 1048592 | tf_op jit(solution)/shard_map/all_gather | solution.py:22
  39.7 0.0 copy-done
  39.7 2.1 convolution_convert_fusion.2
  41.7 26.9 %all-gather.5.cloned.1.call-done = bf16[4096,128]{1,0:T(8,128)(2,1)} async-done(((bf16[1024,128]{1,0:T(8,128)(2,1)}), bf16[4096,128]{1,0:T(8,128)(2,1)}) %all-gather.5.cloned.1.call-update) | async-done | bytes 1048592 | tf_op jit(solution)/shard_map/all_gather | solution.py:21
  68.6 2.0 convolution_convert_fusion.3
  70.7 0.1 copy.34
  70.8 0.6 gather_fusion
  71.4 0.7 broadcast_select_fusion
  72.1 3.3 %all-to-all-start.1 = ((bf16[4,2,32,256]{3,2,1,0:T(8,128)(2,1)}), bf16[4,2,32,256]{3,2,1,0:T(8,128)(2,1)S(1)}, u32[]{:S(2)}, u32[]{:S(2)}) async-start(bf16[4,2,32,256]{3,2,1,0:T(8,128)(2,1)} %broadcast_select_fusion), calls=%async_computation.1 | async-start | bytes 262144 | tf_op jit(solution)/shard_map/all_to_all | solution.py:47
  75.4 0.1 broadcast_compare_fusion.1
  75.5 6.1 %all-to-all-done.1 = bf16[4,2,32,256]{3,2,1,0:T(8,128)(2,1)S(1)} async-done(((bf16[4,2,32,256]{3,2,1,0:T(8,128)(2,1)}), bf16[4,2,32,256]{3,2,1,0:T(8,128)(2,1)S(1)}, u32[]{:S(2)}, u32[]{:S(2)}) %all-to-all-start.1) | async-done | bytes 131104 | tf_op jit(solution)/shard_map/all_to_all | solution.py:47
  81.6 2.1 gather_fusion.1
  83.7 66.7 %all-gather.9.cloned.1.call-done = bf16[4096,512]{1,0:T(8,128)(2,1)} async-done(((bf16[1024,512]{1,0:T(8,128)(2,1)}), bf16[4096,512]{1,0:T(8,128)(2,1)}) %all-gather.9.cloned.1.call-update) | async-done | bytes 4194320 | tf_op jit(solution)/shard_map/all_gather | solution.py:20
  150.3 3.4 %convolution_convert_fusion.1 = bf16[256,512]{1,0:T(8,128)(2,1)S(1)} fusion(bf16[256,4096]{1,0:T(8,128)(2,1)S(1)} %copy-done, bf16[4096,512]{1,0:T(8,128)(2,1)} %all-gather.9.cloned.1.call-done), kind=kOutput, calls=%fused_computation.12 | convolution fusion | flops 1073872896 | bytes 6553600 | tf_op jit(solution)/shard_map/dot_general | solution.py:18
  153.8 0.1 reshape.146
  153.8 2.9 %fusion.2 = (f32[8,4,32]{2,1,0:T(4,128)S(1)}, f32[8,16,32,32,4]{3,2,4,1,0:T(8,128)S(1)}) fusion(pred[8,32,16,32]{1,3,2,0:T(8,128)(4,1)S(1)} %compare_and_fusion, bf16[8,32,4,128,1]{3,2,1,0,4:T(4,128)(2,1)S(1)} %bitcast.88, bf16[8,16,32,256]{3,2,1,0:T(8,128)(2,1)} %bitcast.80), kind=kOutput, calls=%fused_computation.6 | convolution fusion | flops 135789568 | bytes 3543040 | tf_op jit(solution)/shard_map/jqhd,jnbd->jhqnb/dot_general | solution.py:62
  156.8 0.0 copy-start.1
  156.8 2.5 %fusion = f32[8,4,32]{2,1,0:T(4,128)S(1)} fusion(f32[8,16,32,32,4]{3,2,4,1,0:T(8,128)S(1)} %get-tuple-element.19, f32[8,4,32]{2,1,0:T(4,128)S(1)} %get-tuple-element.18, pred[8,32,16,32]{1,3,2,0:T(8,128)(4,1)S(1)} %compare_and_fusion), kind=kLoop, calls=%fused_computation.4 | loop fusion | flops 2096128 | bytes 2236416 | tf_op jit(solution)/shard_map/reduce_sum | solution.py:73
  159.3 0.0 copy-done.1
  159.3 2.2 fusion.16
  161.5 0.1 copy.38
  161.7 2.2 all_gather.18
  163.9 67.1 %all-gather.11.cloned.1.call-done = bf16[1024,2048]{1,0:T(8,128)(2,1)} async-done(((bf16[256,2048]{1,0:T(8,128)(2,1)}), bf16[1024,2048]{1,0:T(8,128)(2,1)}) %all-gather.11.cloned.1.call-update) | async-done | bytes 4194320 | tf_op jit(solution)/shard_map/all_gather | solution.py:87
  231.0 4.4 %convolution_convert_fusion = bf16[256,2048]{1,0:T(8,128)(2,1)} fusion(bf16[256,1024]{1,0:T(8,128)(2,1)S(1)} %all_gather.18, bf16[1024,2048]{1,0:T(8,128)(2,1)} %all-gather.11.cloned.1.call-done), kind=kOutput, calls=%fused_computation.9 | convolution fusion | flops 1074266112 | bytes 5767168 | tf_op jit(solution)/shard_map/dot_general | solution.py:85
  (14 shorter events, 0.2 us)
Async XLA Ops:
  6.5 33.1 %copy-start = (bf16[256,4096]{1,0:T(8,128)(2,1)S(1)}, bf16[256,4096]{1,0:T(8,128)(2,1)}, u32[]{:S(2)}) copy-start(bf16[256,4096]{1,0:T(8,128)(2,1)} %param.7) | copy-start | bytes 6291460
  6.5 33.1 %all-gather.7.cloned.1.call-start = ((), (), s32[]{:S(2)}) async-start(), calls=%async_computation.3 | async-start | bytes 1310720 | tf_op jit(solution)/shard_map/all_gather | solution.py:22
  7.3 61.4 %all-gather.5.cloned.1.call-start = ((), (), s32[]{:S(2)}) async-start(), calls=%async_computation.2 | async-start | bytes 1310720 | tf_op jit(solution)/shard_map/all_gather | solution.py:21
  8.0 142.3 %all-gather.9.cloned.1.call-start = ((), (), s32[]{:S(2)}) async-start(), calls=%async_computation.4 | async-start | bytes 5242880 | tf_op jit(solution)/shard_map/all_gather | solution.py:20
  8.7 222.2 %all-gather.11.cloned.1.call-start = ((), (), s32[]{:S(2)}) async-start(), calls=%async_computation.5 | async-start | bytes 5242880 | tf_op jit(solution)/shard_map/all_gather | solution.py:87
  12.3 11.9 %all-to-all-start = ((s32[4,1,2]{2,1,0:T(1,128)}), s32[4,1,2]{2,1,0:T(1,128)S(1)}, u32[]{:S(2)}, u32[]{:S(2)}) async-start(s32[4,1,2]{2,1,0:T(1,128)} %copy.33), calls=%async_computation | async-start | bytes 4096 | tf_op jit(solution)/shard_map/all_to_all | solution.py:44
  72.1 9.5 %all-to-all-start.1 = ((bf16[4,2,32,256]{3,2,1,0:T(8,128)(2,1)}), bf16[4,2,32,256]{3,2,1,0:T(8,128)(2,1)S(1)}, u32[]{:S(2)}, u32[]{:S(2)}) async-start(bf16[4,2,32,256]{3,2,1,0:T(8,128)(2,1)} %broadcast_select_fusion), calls=%async_computation.1 | async-start | bytes 262144 | tf_op jit(solution)/shard_map/all_to_all | solution.py:47
  156.8 2.6 %copy-start.1 = (bf16[128,32,256]{2,1,0:T(8,128)(2,1)S(1)}, bf16[128,32,256]{2,1,0:T(8,128)(2,1)}, u32[]{:S(2)}) copy-start(bf16[128,32,256]{2,1,0:T(8,128)(2,1)} %gather_fusion.1) | copy-start | bytes 6291460
Sparse Core Ops, SparseCore 0:
  8.9 30.7 all-gather.6
  41.2 27.3 all-gather.4
  70.2 80.1 all-gather.8
  151.8 79.1 all-gather.10
where the time goes:
time: 242 us
  waiting for transfers between devices  187 us (77%)
  matrix products  17 us (7%)
  between operations  14 us (6%)
  starting transfers between devices  9.79 us (4%)
  other arithmetic  7.6 us (3%)
  local copies, waits for them, and re-layouts  4 us (2%)
    all_gather x1, waiting for transfers between devices, body(): lax.all_gather(out_weight, 'kv', axis=0, tiled=True)  67.1 us
    all_gather x1, waiting for transfers between devices, body(): queries = add_rows(lax.all_gather(query_weight, 'kv', axis=0, tiled=True))  66.7 us
    all_gather x1, waiting for transfers between devices, body(): keys = add_rows(lax.all_gather(key_weight, 'kv', axis=0, tiled=True))  26.9 us
    all_gather x1, waiting for transfers between devices, body(): values = add_rows(lax.all_gather(value_weight, 'kv', axis=0, tiled=True))  15.4 us
    dot_general x3, matrix products, add_rows(): return jnp.dot(tokens, piece, preferred_element_type=jnp.float32)  7.53 us
    all_to_all x1, starting transfers between devices, body(): lax.all_to_all(wanted, 'kv', split_axis=0, concat_axis=0, tiled=True)  6.35 us
    all_to_all x1, waiting for transfers between devices, body(): lax.all_to_all(outgoing, 'kv', split_axis=0, concat_axis=0, tiled=True)  6.06 us
  transfers between devices with their start and end apart: 6, of which 6 were waited for; matrix products, arithmetic and copies ran while one was open for 10% of the time, Pallas kernels for 0%

commit v1 on v0

--- a/solution.py
+++ b/solution.py
@@ -1,14 +1,19 @@
+import functools
+
 import jax
 import jax.numpy as jnp
 from jax import lax
+from jax.experimental import pallas as pl
+from jax.experimental.pallas import tpu as pltpu
 from jax.sharding import PartitionSpec as P
 
 HD = 128
 BLOCK = 32
 CAP = 2
-
-
-def body(tokens, query_weight, key_weight, value_weight, out_weight, chosen, live_length):
+MESH = pl.DeviceIdType.MESH
+
+
+def gathered_body(tokens, query_weight, key_weight, value_weight, out_weight, chosen, live_length):
     rows = tokens.shape[0]
     per_dev = rows // BLOCK
     owners = lax.axis_size("kv")
@@ -90,6 +95,309 @@
     return mixed.astype(jnp.bfloat16)
 
 
+class Stream:
+    def __init__(self, place, full, first, rows, halved, sends, recvs, base):
+        self.place, self.full, self.halved = place, full, halved
+        self.shard = full.shape[0] // place["n"]
+        self.first, self.rows = first, rows
+        self.sends, self.recvs, self.base = sends, recvs, base
+        self.begun = []
+
+    def part(self, owner, index, count):
+        size = self.rows // count
+        start = pl.multiple_of(owner * self.shard + self.first + index * size, size)
+        return self.full.at[pl.ds(start, size), :]
+
+    def carried(self, owner):
+        if self.halved:
+            return self.part(owner, self.place["half"], 2)
+        return self.part(owner, self.place["dp"], 4)
+
+    def copy(self, part, owner, kind, target, sent_as=None):
+        at = self.base + owner * 5
+        return pltpu.make_async_remote_copy(
+            src_ref=part,
+            dst_ref=part,
+            send_sem=self.sends.at[at + (kind if sent_as is None else sent_as)],
+            recv_sem=self.recvs.at[at + kind],
+            device_id=target,
+            device_id_type=MESH,
+        )
+
+    def begin(self, c, when=None):
+        if when is None:
+            c.start()
+        else:
+            pl.when(when)(c.start)
+        self.begun.append((c, when))
+
+    def issue(self):
+        p = self.place
+        me, n = p["me"], p["n"]
+        mine = self.carried(me)
+        self.begin(self.copy(mine, me, 0, {"kv": p["right"]}), me < n - 1)
+        self.begin(self.copy(mine, me, 0, {"kv": p["left"]}, 1), me > 0)
+
+    def relay(self, slot):
+        p = self.place
+        me, n, owner = p["me"], p["n"], p["order"][slot]
+        piece = self.carried(owner)
+        self.copy(piece, owner, 0, {"kv": p["right"]}).wait_recv()
+        self.begin(
+            self.copy(piece, owner, 0, {"kv": p["right"]}), jnp.logical_and(owner < me, me < n - 1)
+        )
+        self.begin(self.copy(piece, owner, 0, {"kv": p["left"]}, 0), jnp.logical_and(owner > me, me > 0))
+        if self.halved:
+            to_x = self.part(owner, 2 * p["half"], 4)
+            to_y = self.part(owner, 2 * p["half"] + 1, 4)
+        else:
+            to_x = to_y = piece
+        self.begin(self.copy(to_x, owner, 1, {"dp": p["x"]}))
+        self.begin(self.copy(to_y, owner, 2, {"dp": p["y"]}))
+
+    def corner(self, slot):
+        p = self.place
+        owner = p["order"][slot]
+        if self.halved:
+            other = 2 * (1 - p["half"])
+            self.copy(self.part(owner, other, 4), owner, 1, {"dp": p["x"]}).wait_recv()
+            self.copy(self.part(owner, other + 1, 4), owner, 2, {"dp": p["y"]}).wait_recv()
+            return
+        self.copy(self.part(owner, p["x"], 4), owner, 1, {"dp": p["x"]}).wait_recv()
+        self.begin(self.copy(self.part(owner, 2 * p["x"], 8), owner, 4, {"dp": p["y"]}))
+        self.copy(self.part(owner, p["y"], 4), owner, 2, {"dp": p["y"]}).wait_recv()
+        self.begin(self.copy(self.part(owner, 2 * p["y"] + 1, 8), owner, 3, {"dp": p["x"]}))
+
+    def arrive(self):
+        p = self.place
+        if self.halved:
+            return
+        for owner in p["order"]:
+            self.copy(self.part(owner, 2 * p["far"], 8), owner, 4, {"dp": p["y"]}).wait_recv()
+            self.copy(self.part(owner, 2 * p["far"] + 1, 8), owner, 3, {"dp": p["x"]}).wait_recv()
+
+    def finish(self):
+        for c, when in self.begun:
+            if when is None:
+                c.wait_send()
+            else:
+                pl.when(when)(c.wait_send)
+
+
+def kernel(
+    n, chosen, live, tokens, query_w, key_w, value_w, out_w, mixed,
+    tok, full_q, full_k, full_v, full_o, paired, queries, bias, attended,
+    local_sem, send_sem, recv_sem, kv_send, kv_recv, tp_send, tp_recv,
+):
+    dp, me, tp = lax.axis_index("dp"), lax.axis_index("kv"), lax.axis_index("tp")
+    x_at, y_at = lax.rem(dp, 2), lax.div(dp, 2)
+    place = {
+        "n": n,
+        "me": me,
+        "left": lax.rem(me + n - 1, n),
+        "right": lax.rem(me + 1, n),
+        "opp": lax.rem(me + 2, n),
+        "x": 2 * y_at + (1 - x_at),
+        "y": 2 * (1 - y_at) + x_at,
+        "half": lax.rem(x_at + y_at, 2),
+        "dp": dp,
+        "far": 2 * (1 - y_at) + (1 - x_at),
+    }
+    order = []
+    for i in range(n - 1):
+        up = i + (i >= me).astype(jnp.int32)
+        down = n - 1 - i - (n - 1 - i <= me).astype(jnp.int32)
+        order.append(jnp.where(2 * me < n, up, down))
+    place["order"] = order
+    rows = tok.shape[0]
+    per_dev = rows // BLOCK
+    seq = n * rows
+
+    fulls = (full_k, full_v, full_q, full_o)
+    loads = []
+    for index, (shard, full) in enumerate(zip((key_w, value_w, query_w, out_w), fulls)):
+        size = shard.shape[0]
+        mine = full.at[pl.ds(pl.multiple_of(me * size, size), size), :]
+        loads.append(pltpu.make_async_copy(shard, mine, local_sem.at[index]))
+    loads.append(pltpu.make_async_copy(tokens, tok, local_sem.at[4]))
+    for load in loads:
+        load.start()
+
+    barrier = pltpu.get_barrier_semaphore()
+    greeted = [{"kv": place[k]} for k in ("left", "right", "opp")]
+    greeted += [{"dp": place[k]} for k in ("x", "y")] + [{"tp": 1 - tp}]
+    for target in greeted:
+        pl.semaphore_signal(barrier, inc=1, device_id=target, device_id_type=MESH)
+    pl.semaphore_wait(barrier, len(greeted))
+
+    cut = full_o.shape[0] // n // 2
+    plan = [(full_k, 0, 0), (full_v, 0, 0), (full_q, 0, 0), (full_o, 0, 0), (full_o, cut, 1)]
+    streams = []
+    for i, (full, first, halved) in enumerate(plan):
+        count = cut if full is full_o else full.shape[0] // n
+        streams.append(
+            Stream(place, full, first, count, halved, send_sem, recv_sem, 5 * n * i)
+        )
+    groups = [streams[:2], streams[2:3], streams[3:4], streams[4:5]]
+    each = n - 1
+
+    def advance(at):
+        group, slot = divmod(at, each)
+        if group < len(groups):
+            for s in groups[group]:
+                s.relay(slot)
+            if slot == 0 and group + 1 < len(groups):
+                for s in groups[group + 1]:
+                    s.issue()
+        if at > 0:
+            group, slot = divmod(at - 1, each)
+            for s in groups[group]:
+                s.corner(slot)
+
+    loads[0].wait()
+    loads[1].wait()
+    for s in groups[0]:
+        s.issue()
+    loads[2].wait()
+    loads[3].wait()
+    loads[4].wait()
+
+    column = lax.broadcasted_iota(jnp.int32, (BLOCK, seq), 1)
+    row = lax.broadcasted_iota(jnp.int32, (BLOCK, seq), 0)
+    key_block = lax.div(lax.broadcasted_iota(jnp.int32, (8, seq), 1), BLOCK)
+    for j in range(per_dev):
+        listed = jnp.full((8, seq), -jnp.inf, jnp.float32)
+        for e in range(chosen.shape[1]):
+            listed = jnp.where(key_block == chosen[j, e], 0.0, listed)
+        spread = jnp.concatenate([listed] * (BLOCK // 8), axis=0)
+        causal = column <= row + (me * rows + j * BLOCK)
+        bias[j * BLOCK : (j + 1) * BLOCK, :] = jnp.where(causal, spread, -jnp.inf)
+
+    for at in range(each + 2):
+        advance(at)
+    for s in groups[0]:
+        s.arrive()
+    mine = pl.ds(pl.multiple_of(me * rows, rows), rows)
+    paired[mine, :HD] = jnp.dot(
+        tok[...], full_k[...], preferred_element_type=jnp.float32
+    ).astype(jnp.bfloat16)
+    paired[mine, HD:] = jnp.dot(
+        tok[...], full_v[...], preferred_element_type=jnp.float32
+    ).astype(jnp.bfloat16)
+    advance(each + 2)
+    kv_copies = []
+    for step in range(1, n):
+        block = paired.at[mine, :]
+        c = pltpu.make_async_remote_copy(
+            src_ref=block, dst_ref=block,
+            send_sem=kv_send.at[step - 1], recv_sem=kv_recv.at[step - 1],
+            device_id={"kv": lax.rem(me + step, n)}, device_id_type=MESH,
+        )
+        c.start()
+        kv_copies.append(c)
+    for at in range(each + 3, 2 * each + 2):
+        advance(at)
+    groups[1][0].arrive()
+    queries[...] = jnp.dot(
+        tok[...], full_q[...], preferred_element_type=jnp.float32
+    ).astype(jnp.bfloat16)
+    advance(2 * each + 2)
+    for step in range(1, n):
+        owner = lax.rem(me + n - step, n)
+        block = paired.at[pl.ds(pl.multiple_of(owner * rows, rows), rows), :]
+        pltpu.make_async_remote_copy(
+            src_ref=block, dst_ref=block,
+            send_sem=kv_send.at[step - 1], recv_sem=kv_recv.at[step - 1],
+            device_id={"kv": lax.rem(me + step, n)}, device_id_type=MESH,
+        ).wait_recv()
+
+    position = me * rows + lax.broadcasted_iota(jnp.int32, (rows, HD), 0)
+    alive = position < live[0]
+    heads = queries.shape[1] // HD
+    for h in range(heads):
+        cols = slice(h * HD, (h + 1) * HD)
+        scores = lax.dot_general(
+            queries[:, cols], paired[:, :HD], (((1,), (1,)), ((), ())),
+            preferred_element_type=jnp.float32,
+        )
+        masked = scores * HD ** (-0.5) + bias[...]
+        top = jnp.max(masked, axis=1, keepdims=True)
+        weights = jnp.exp(masked - top)
+        total = jnp.sum(weights, axis=1, keepdims=True)
+        summed = jnp.dot(
+            weights.astype(jnp.bfloat16), paired[:, HD:], preferred_element_type=jnp.float32
+        )
+        result = jnp.where(alive, summed / total, 0.0).astype(jnp.bfloat16)
+        attended[tp, :, cols] = result
+        if h == heads // 2 - 1:
+            advance(2 * each + 3)
+    share = pltpu.make_async_remote_copy(
+        src_ref=attended.at[tp], dst_ref=attended.at[tp],
+        send_sem=tp_send, recv_sem=tp_recv, device_id={"tp": 1 - tp}, device_id_type=MESH,
+    )
+    share.start()
+    for at in range(2 * each + 4, len(groups) * each + 1):
+        advance(at)
+    pltpu.make_async_remote_copy(
+        src_ref=attended.at[1 - tp], dst_ref=attended.at[1 - tp],
+        send_sem=tp_send, recv_sem=tp_recv, device_id={"tp": 1 - tp}, device_id_type=MESH,
+    ).wait_recv()
+    for s in groups[2] + groups[3]:
+        s.arrive()
+    wide = queries.shape[1]
+    tile = 512
+    for c in range(0, mixed.shape[1], tile):
+        acc = jnp.dot(
+            attended[0], full_o[:wide, c : c + tile], preferred_element_type=jnp.float32
+        )
+        acc += jnp.dot(
+            attended[1], full_o[wide:, c : c + tile], preferred_element_type=jnp.float32
+        )
+        mixed[:, c : c + tile] = acc.astype(jnp.bfloat16)
+    for s in streams:
+        s.finish()
+    for c in kv_copies:
+        c.wait_send()
+    share.wait_send()
+
+
+def woven_body(tokens, query_weight, key_weight, value_weight, out_weight, chosen, live_length):
+    n = lax.axis_size("kv")
+    rows, width = tokens.shape
+    wide = query_weight.shape[1]
+    dma = pltpu.SemaphoreType.DMA
+    bf16 = jnp.bfloat16
+    anywhere = pl.BlockSpec(memory_space=pl.ANY)
+    small = pl.BlockSpec(memory_space=pltpu.SMEM)
+    return pl.pallas_call(
+        functools.partial(kernel, n),
+        out_shape=jax.ShapeDtypeStruct((rows, out_weight.shape[1]), bf16),
+        in_specs=[small, small] + [anywhere] * 5,
+        out_specs=pl.BlockSpec(memory_space=pltpu.VMEM),
+        scratch_shapes=[
+            pltpu.VMEM((rows, width), bf16),
+            pltpu.VMEM((width, wide), bf16),
+            pltpu.VMEM((width, HD), bf16),
+            pltpu.VMEM((width, HD), bf16),
+            pltpu.VMEM((n * out_weight.shape[0], out_weight.shape[1]), bf16),
+            pltpu.VMEM((n * rows, 2 * HD), bf16),
+            pltpu.VMEM((rows, wide), bf16),
+            pltpu.VMEM((rows, n * rows), jnp.float32),
+            pltpu.VMEM((2, rows, wide), bf16),
+            dma((5,)),
+            dma((5 * 5 * n,)),
+            dma((5 * 5 * n,)),
+            dma((n - 1,)),
+            dma((n - 1,)),
+            dma,
+            dma,
+        ],
+        compiler_params=pltpu.CompilerParams(
+            collective_id=0, has_side_effects=True, vmem_limit_bytes=56 * 2**20
+        ),
+    )(chosen, live_length, tokens, query_weight, key_weight, value_weight, out_weight)
+
+
 def solution(mesh):
     in_specs = (
         P(("dp", "kv"), None),
@@ -101,4 +409,6 @@
         P("dp"),
     )
     out_specs = P(("dp", "kv"), "tp")
+    fits = (mesh.shape["dp"], mesh.shape["kv"], mesh.shape["tp"]) == (4, 4, 2)
+    body = woven_body if fits else gathered_body
     return jax.shard_map(body, mesh=mesh, in_specs=in_specs, out_specs=out_specs, check_vma=False)

time: 242 us -> 83.7 us (0.35)
  waiting for transfers between devices: 187 us -> 0 us
  Pallas kernels: 0 us -> 80.6 us
  matrix products: 17 us -> 0 us
  between operations: 14 us -> 0.66 us
  starting transfers between devices: 9.79 us -> 0 us
  other arithmetic: 7.6 us -> 0 us
    all_gather x4 -> x0, waiting for transfers between devices: 176 us -> none  [the longest x1 67.1 us: body(): lax.all_gather(out_weight, 'kv', axis=0, tiled=True)]
    pallas_call x0 -> x1, Pallas kernels: none -> 80.6 us  [woven_body(): pl.pallas_call(functools.partial(kernel, n), out_shape=jax.ShapeDtypeStru...]
    dot_general x6 -> x0, matrix products: 17 us -> none  [the longest x3 7.53 us: add_rows(): return jnp.dot(tokens, piece, preferred_element_type=jnp.float32)]
    all_to_all x2 -> x0, starting transfers between devices: 9.67 us -> none  [the longest x1 6.35 us: body(): lax.all_to_all(wanted, 'kv', split_axis=0, concat_axis=0, tiled=True)]
    all_to_all x2 -> x0, waiting for transfers between devices: 8.74 us -> none  [the longest x1 6.06 us: body(): lax.all_to_all(outgoing, 'kv', split_axis=0, concat_axis=0, tiled=True)]
    reduce_sum x3 -> x0, other arithmetic: 2.81 us -> none  [the longest x1 2.53 us: body(): total = jnp.sum(weights, axis=(3, 4))]
    gather x2 -> x0, local copies, waits for them, and re-layouts: 2.63 us -> none  [the longest x1 2.07 us: body(): picked = table[position]]
    unnamed x4 -> x0, waiting for transfers between devices: 2.61 us -> none
  transfers between devices with their start and end apart: 6 -> 0, of which waited for: 6 -> 0; matrix products, arithmetic and copies ran while one was open for 10% -> 0% of each run, Pallas kernels for 0% -> 0%
where the time goes in v1:
time: 83.7 us; the launch traced here: 83.5 us
  Pallas kernels  80.6 us (96%)
  local copies, waits for them, and re-layouts  2.3 us (3%)
    pallas_call x1, Pallas kernels, woven_body(): pl.pallas_call(functools.partial(kernel, n), out_shape=jax.ShapeDtypeStru...  80.6 us
    unnamed x1, local copies, waits for them, and re-layouts  2.3 us

profile of v1, /device:TPU:0, one launch (start us, length us, event | category | flops | bytes accessed | tf_op | source)
XLA Modules:
  0.0 83.5 jit_solution(12765777763426688900)
XLA Ops:
  0.7 80.6 %shard_map.73 = bf16[256,2048]{1,0:T(8,128)(2,1)} custom-call(s32[8,16]{1,0:T(8,128)} %chosen.1, s32[1]{0:T(128)S(6)} %copy.9.live, bf16[256,4096]{1,0:T(8,128)(2,1)} %tokens.1, bf16[1024,512]{1,0:T(8,128)(2,1)} %query_w.1, bf16[1024,128]{1,0:T(8,128)(2,1)} %key_w.1, bf16[1024,128]{1,0:T(8,128)(2,1)} %value_w.1, bf16[256,2048]{1,0:T(8,128)(2,1)} %out_w.1), custom_call_target="tpu_custom_call" | custom-call | tf_op jit(solution)/shard_map/pallas_call | solution.py:372
  81.2 2.3 %copy.10 = bf16[256,2048]{1,0:T(8,128)(2,1)} copy(bf16[256,2048]{1,0:T(8,128)(2,1)} %shard_map.73) | data formatting | bytes 2097152
